TPU v7x, 32 devices: a whole 2x2x4 slice. The times are simulated.
32 devices in a mesh: fs: 8 (over z, x), tp: 4 (over y, core).
Axes of the slice: x: 2, y: 2, z: 4, core: 2. Of those that a mesh axis runs over, the one named last changes fastest.
Arguments:
- later_input: bfloat16 [4096, 2048], P(('fs', 'tp')), may hold values from -6 to 6
- saved_input: bfloat16 [4096, 2048], P(('fs', 'tp')), may hold values from -6 to 6
- cotangent: bfloat16 [4096, 3072], P('fs', 'tp'), may hold values from -6 to 6
- up_weight: bfloat16 [2048, 3072], P('fs', 'tp'), may hold values from -0.125 to 0.125
- gate_weight: bfloat16 [2048, 3072], P('fs', 'tp'), may hold values from -0.125 to 0.125
- up_taps: bfloat16 [3, 3072], replicated, may hold values from -3.5 to 3.5
- gate_taps: bfloat16 [3, 3072], replicated, may hold values from -3.5 to 3.5
- up_grad_sum: float32 [2048, 3072], P('fs', 'tp'), may hold values from -6 to 6
- gate_grad_sum: float32 [2048, 3072], P('fs', 'tp'), may hold values from -6 to 6
- up_taps_sum: float32 [3, 3072], replicated, may hold values from -6 to 6
- gate_taps_sum: float32 [3, 3072], replicated, may hold values from -6 to 6
Outputs:
- hidden: bfloat16 [4096, 3072], P('fs', 'tp')
- input_grad: bfloat16 [4096, 2048], P(('fs', 'tp'))
- new_up_sum: float32 [2048, 3072], P('fs', 'tp')
- new_gate_sum: float32 [2048, 3072], P('fs', 'tp')
- new_up_taps_sum: float32 [3, 3072], replicated
- new_gate_taps_sum: float32 [3, 3072], replicated
All inputs are finite; a program needn't handle non-finite values.
Results may differ from a plain program's by a relative error of at most 0.018.
Values may be sent and summed in bfloat16 or wider, within the bound.
A program may use at most 64 MiB of HBM per device.

v0:
```python
import jax
import jax.numpy as jnp
from jax import lax
from jax.sharding import PartitionSpec as P


def delayed(values, steps):
    zeros = jnp.zeros_like(values[:steps])
    return jnp.concatenate([zeros, values[:-steps]], axis=0)


def advanced(values, steps):
    zeros = jnp.zeros_like(values[:steps])
    return jnp.concatenate([values[steps:], zeros], axis=0)


def depthwise(values, taps):
    return taps[2] * values + taps[1] * delayed(values, 1) + taps[0] * delayed(values, 2)


def depthwise_back(grads, taps):
    return taps[2] * grads + taps[1] * advanced(grads, 1) + taps[0] * advanced(grads, 2)


def taps_grad(grads, values):
    return jnp.stack(
        [
            jnp.sum(grads * delayed(values, 2), axis=0),
            jnp.sum(grads * delayed(values, 1), axis=0),
            jnp.sum(grads * values, axis=0),
        ],
        axis=0,
    )


def make_term(rows_all, grads):
    return lax.dot_general(
        rows_all, grads, (((0,), (0,)), ((), ())), preferred_element_type=jnp.float32
    )


def shards(
    later_input,
    saved_input,
    cotangent,
    up_weight,
    gate_weight,
    up_taps,
    gate_taps,
    up_grad_sum,
    gate_grad_sum,
    up_taps_sum,
    gate_taps_sum,
):
    column_count = up_weight.shape[1]
    group_size = lax.axis_size("tp")
    offset = lax.axis_index("tp") * column_count
    tokens_all = later_input.shape[0] * lax.axis_size("fs") * group_size
    grad_scale = jnp.float32(tokens_all ** (-0.5))
    taps_both = jnp.concatenate(
        [
            lax.dynamic_slice_in_dim(up_taps, offset, column_count, 1),
            lax.dynamic_slice_in_dim(gate_taps, offset, column_count, 1),
        ],
        axis=1,
    ).astype(jnp.float32)
    weight_both = jnp.concatenate([up_weight, gate_weight], axis=1)
    later_rows = lax.all_gather(later_input, "tp", axis=0, tiled=True)
    saved_rows = lax.all_gather(saved_input, "tp", axis=0, tiled=True)
    shard_rows = lax.all_gather(weight_both, "fs", axis=0, tiled=True)
    proj_later = jnp.dot(later_rows, shard_rows, preferred_element_type=jnp.float32)
    proj_saved = jnp.dot(saved_rows, shard_rows, preferred_element_type=jnp.float32)
    conv_later = depthwise(proj_later.astype(jnp.bfloat16).astype(jnp.float32), taps_both)
    hidden = (jax.nn.silu(conv_later[:, column_count:]) * conv_later[:, :column_count]).astype(
        jnp.bfloat16
    )
    saved_proj = proj_saved.astype(jnp.bfloat16)
    saved_proj32 = saved_proj.astype(jnp.float32)
    conv_saved = depthwise(saved_proj32, taps_both)
    saved_up = conv_saved[:, :column_count]
    saved_gate = conv_saved[:, column_count:]
    sigmoid_gate = jax.nn.sigmoid(saved_gate)
    upstream = cotangent.astype(jnp.float32)
    grad_conv = jnp.concatenate(
        [
            upstream * jax.nn.silu(saved_gate),
            upstream * saved_up * sigmoid_gate * (1.0 + saved_gate * (1.0 - sigmoid_gate)),
        ],
        axis=1,
    )
    grad_proj = depthwise_back(grad_conv, taps_both).astype(jnp.bfloat16)
    taps_local = taps_grad(grad_conv, saved_proj32)
    total_cols = column_count * group_size
    taps_up_full = lax.dynamic_update_slice_in_dim(
        jnp.zeros((3, total_cols), jnp.float32), taps_local[:, :column_count], offset, 1
    )
    taps_gate_full = lax.dynamic_update_slice_in_dim(
        jnp.zeros((3, total_cols), jnp.float32), taps_local[:, column_count:], offset, 1
    )
    taps_up_total, taps_gate_total = lax.psum((taps_up_full, taps_gate_full), ("fs", "tp"))
    weight_grad = lax.psum_scatter(
        make_term(saved_rows, grad_proj).astype(jnp.bfloat16), "fs", scatter_dimension=0, tiled=True
    ).astype(jnp.float32)
    up_grad = weight_grad[:, :column_count]
    gate_grad = weight_grad[:, column_count:]
    partial_grad = lax.dot_general(
        grad_proj,
        lax.all_gather(weight_both, "fs", axis=0, tiled=True),
        (((1,), (1,)), ((), ())),
        preferred_element_type=jnp.float32,
    )
    input_grad = lax.psum_scatter(
        partial_grad.astype(jnp.bfloat16), "tp", scatter_dimension=0, tiled=True
    )
    new_up_sum = up_grad_sum + grad_scale * up_grad
    new_gate_sum = gate_grad_sum + grad_scale * gate_grad
    new_up_taps_sum = up_taps_sum + grad_scale * taps_up_total
    new_gate_taps_sum = gate_taps_sum + grad_scale * taps_gate_total
    return (hidden, input_grad, new_up_sum, new_gate_sum, new_up_taps_sum, new_gate_taps_sum)


def solution(mesh):
    return jax.shard_map(
        shards,
        mesh=mesh,
        in_specs=(
            P(("fs", "tp"), None),
            P(("fs", "tp"), None),
            P("fs", "tp"),
            P("fs", "tp"),
            P("fs", "tp"),
            P(),
            P(),
            P("fs", "tp"),
            P("fs", "tp"),
            P(),
            P(),
        ),
        out_specs=(P("fs", "tp"), P(("fs", "tp"), None), P("fs", "tp"), P("fs", "tp"), P(), P()),
        check_vma=False,
    )
```

profile of v0, /device:TPU:0, one launch (start us, length us, event | category | flops | bytes accessed | tf_op | source)
XLA Modules:
  0.0 459.7 jit_solution(4171032246797810518)
XLA Ops:
  7.2 0.7 all-gather.8.cloned.1.call-update
  8.0 2.0 pad_maximum_fusion.1
  10.1 0.7 all-gather.6.cloned.1.call-update
  10.8 1.2 copy.17
  12.0 0.7 constant_dynamic-slice_fusion
  12.8 22.1 %all-gather.8.cloned.1.call-done = bf16[512,2048]{1,0:T(8,128)(2,1)} async-done(((bf16[128,2048]{1,0:T(8,128)(2,1)}), bf16[512,2048]{1,0:T(8,128)(2,1)}) %all-gather.8.cloned.1.call-update) | async-done | bytes 2097168 | tf_op jit(solution)/shard_map/all_gather | solution.py:69
  34.9 101.5 %all-gather.4.cloned.1.call-done = bf16[2048,1536]{1,0:T(8,128)(2,1)} async-done(((bf16[256,1536]{1,0:T(8,128)(2,1)}), bf16[2048,1536]{1,0:T(8,128)(2,1)}) %all-gather.4.cloned.1.call-update) | async-done | bytes 6291472 | tf_op jit(solution)/shard_map/all_gather | solution.py:70
  136.3 6.2 %convert_bitcast_fusion = f32[512,1536]{0,1:T(8,128)S(1)} fusion(bf16[2048,1536]{1,0:T(8,128)(2,1)} %all-gather.4.cloned.1.call-done, bf16[512,2048]{1,0:T(8,128)(2,1)} %all-gather.8.cloned.1.call-done), kind=kOutput, calls=%fused_computation.9 | convolution fusion | flops 3222798336 | bytes 11534336 | tf_op jit(solution)/shard_map/dot_general | solution.py:72
  142.6 2.6 multiply_add_fusion
  145.3 0.9 fusion.4
  146.2 2.7 fusion.1
  149.0 2.6 fusion.2
  151.6 7.1 %all-gather.6.cloned.1.call-done = bf16[512,2048]{1,0:T(8,128)(2,1)} async-done(((bf16[128,2048]{1,0:T(8,128)(2,1)}), bf16[512,2048]{1,0:T(8,128)(2,1)}) %all-gather.6.cloned.1.call-update) | async-done | bytes 2097168 | tf_op jit(solution)/shard_map/all_gather | solution.py:68
  158.7 6.4 %convert_bitcast_fusion.1 = f32[512,1536]{0,1:T(8,128)S(1)} fusion(bf16[2048,1536]{1,0:T(8,128)(2,1)} %all-gather.4.cloned.1.call-done, bf16[512,2048]{1,0:T(8,128)(2,1)} %all-gather.6.cloned.1.call-done), kind=kOutput, calls=%fused_computation.10 | convolution fusion | flops 3222798336 | bytes 11534336 | tf_op jit(solution)/shard_map/dot_general | solution.py:71
  165.1 7.4 %multiply_reduce_fusion.2 = (f32[1536]{0:T(1024)S(1)}, f32[1536]{0:T(1024)S(1)}, f32[1536]{0:T(1024)S(1)}, bf16[512,1536]{0,1:T(8,128)(2,1)}, f32[512,1536]{0,1:T(8,128)}) fusion(f32[510,1536]{0,1:T(8,128)S(1)} %bitcast.20, f32[512,768]{0,1:T(8,128)S(1)} %copy-done.1, f32[512,768]{0,1:T(8,128)S(1)} %copy-done.3, f32[512,1536]{0,1:T(8,128)S(1)} %convert_bitcast_fusion, ...), kind=kLoop, calls=%fused_computation.13 | loop fusion | flops 14151168 | bytes 33011712 | tf_op jit(solution)/shard_map/reduce_sum | solution.py:28
  172.7 0.6 copy-done.13
  173.3 0.2 reduce-scatter.5.cloned.1.call-start
  173.6 8.2 %fusion = bf16[2048,1536]{0,1:T(8,128)(2,1)} fusion(bf16[512,1536]{0,1:T(8,128)(2,1)} %get-tuple-element.22, bf16[512,2048]{1,0:T(8,128)(2,1)} %all-gather.8.cloned.1.call-done), kind=kOutput, calls=%fused_computation.1 | convolution fusion | flops 3224371200 | bytes 9961472 | tf_op jit(solution)/shard_map/dot_general | solution.py:37
  181.9 1.3 copy-done.10
  183.2 7.6 %convolution_convert_fusion.1 = bf16[512,2048]{1,0:T(8,128)(2,1)} fusion(bf16[512,1536]{0,1:T(8,128)(2,1)S(1)} %copy-done.10, bf16[2048,1536]{1,0:T(8,128)(2,1)} %all-gather.4.cloned.1.call-done), kind=kOutput, calls=%fused_computation.17 | convolution fusion | flops 3222274048 | bytes 9961472 | tf_op jit(solution)/shard_map/dot_general | solution.py:106
  190.8 2.5 copy.19
  193.2 2.3 copy.20
  195.5 1.4 fusion.5
  196.9 2.4 copy.21
  199.3 97.3 %all-reduce.9.cloned.1.call-done = (f32[3,3072]{1,0:T(4,128)}, f32[3,3072]{1,0:T(4,128)}) async-done(((f32[3,3072]{1,0:T(4,128)}, f32[3,3072]{1,0:T(4,128)}), (f32[3,3072]{1,0:T(4,128)}, f32[3,3072]{1,0:T(4,128)})) %all-reduce.9.cloned.1.call-update) | async-done | bytes 73744 | tf_op jit(solution)/shard_map/psum | solution.py:100
  296.6 1.4 multiply_add_fusion.2
  298.0 1.4 multiply_add_fusion.3
  299.5 120.0 %reduce-scatter.5.cloned.1.call-done = bf16[256,1536]{0,1:T(8,128)(2,1)} async-done(((bf16[2048,1536]{0,1:T(8,128)(2,1)}), bf16[256,1536]{0,1:T(8,128)(2,1)}) %reduce-scatter.5.cloned.1.call-update) | async-done | bytes 786448 | tf_op jit(solution)/shard_map/reduce_scatter | solution.py:101
  419.5 1.2 convert_element_type.57
  421.0 1.1 copy.22
  422.1 1.1 copy.23
  423.3 29.6 %reduce-scatter.3.cloned.1.call-done = bf16[128,2048]{1,0:T(8,128)(2,1)} async-done(((bf16[512,2048]{1,0:T(8,128)(2,1)}), bf16[128,2048]{1,0:T(8,128)(2,1)}) %reduce-scatter.3.cloned.1.call-update) | async-done | bytes 524304 | tf_op jit(solution)/shard_map/reduce_scatter | solution.py:112
  (49 shorter events, 0.7 us)
Async XLA Ops:
  7.2 3.7 copy-start.11
  7.2 27.7 %all-gather.8.cloned.1.call-start = ((), (), s32[]{:S(2)}) async-start(), calls=%async_computation.4 | async-start | bytes 2621440 | tf_op jit(solution)/shard_map/all_gather | solution.py:69
  7.9 128.4 %all-gather.4.cloned.1.call-start = ((), (), s32[]{:S(2)}) async-start(), calls=%async_computation.2 | async-start | bytes 7077888 | tf_op jit(solution)/shard_map/all_gather | solution.py:70
  10.0 148.7 %all-gather.6.cloned.1.call-start = ((), (), s32[]{:S(2)}) async-start(), calls=%async_computation.3 | async-start | bytes 2621440 | tf_op jit(solution)/shard_map/all_gather | solution.py:68
  10.8 285.8 %all-reduce.9.cloned.1.call-start = ((), (), s32[]{:S(2)}) async-start(), calls=%async_computation.7 | async-start | bytes 196608 | tf_op jit(solution)/shard_map/psum | solution.py:100
  142.6 2.7 copy-start.9
  146.2 2.8 copy-start
  146.2 2.7 copy-start.2
  158.7 6.4 %copy-start.1 = (f32[512,768]{0,1:T(8,128)S(1)}, f32[512,768]{0,1:T(8,128)}, u32[]{:S(2)}) copy-start(f32[512,768]{0,1:T(8,128)} %copy-done) | copy-start | bytes 4718596
  158.7 6.4 %copy-start.3 = (f32[512,768]{0,1:T(8,128)S(1)}, f32[512,768]{0,1:T(8,128)}, u32[]{:S(2)}) copy-start(f32[512,768]{0,1:T(8,128)} %copy-done.2) | copy-start | bytes 4718596
  158.7 6.4 %copy-start.4 = (f32[511,1536]{0,1:T(8,128)S(1)}, f32[511,1536]{0,1:T(8,128)}, u32[]{:S(2)}) copy-start(f32[511,1536]{0,1:T(8,128)} %fusion.1) | copy-start | bytes 9418756
  158.7 6.4 %copy-start.5 = (f32[510,1536]{0,1:T(8,128)S(1)}, f32[510,1536]{0,1:T(8,128)}, u32[]{:S(2)}) copy-start(f32[510,1536]{0,1:T(8,128)} %fusion.2) | copy-start | bytes 9400324
  172.7 0.6 copy-start.13
  172.7 0.6 copy-start.12
  173.3 246.1 %reduce-scatter.5.cloned.1.call-start = ((), (), s32[]{:S(2)}) async-start(), calls=%async_computation.6 | async-start | bytes 7077888 | tf_op jit(solution)/shard_map/reduce_scatter | solution.py:101
  181.8 1.4 copy-start.10
  181.8 271.1 %reduce-scatter.3.cloned.1.call-start = ((), (), s32[]{:S(2)}) async-start(), calls=%async_computation.5 | async-start | bytes 2621440 | tf_op jit(solution)/shard_map/reduce_scatter | solution.py:112
  190.7 4.8 %copy-start.6 = (f32[512,1536]{0,1:T(8,128)S(1)}, f32[512,1536]{0,1:T(8,128)}, u32[]{:S(2)}) copy-start(f32[512,1536]{0,1:T(8,128)} %get-tuple-element.25) | copy-start | bytes 9437188
  195.5 101.1 %copy-start.14 = (f32[3,3072]{1,0:T(4,128)S(1)}, f32[3,3072]{1,0:T(4,128)}, u32[]{:S(2)}) copy-start(f32[3,3072]{1,0:T(4,128)} %param.21) | copy-start | bytes 110596
  195.5 102.5 %copy-start.15 = (f32[3,3072]{1,0:T(4,128)S(1)}, f32[3,3072]{1,0:T(4,128)}, u32[]{:S(2)}) copy-start(f32[3,3072]{1,0:T(4,128)} %param.20) | copy-start | bytes 110596
  196.9 223.8 %copy-start.7 = (f32[256,768]{0,1:T(8,128)S(1)}, f32[256,768]{0,1:T(8,128)}, u32[]{:S(2)}) copy-start(f32[256,768]{0,1:T(8,128)} %copy.19) | copy-start | bytes 2359300
  196.9 223.9 %copy-start.8 = (f32[256,768]{0,1:T(8,128)S(1)}, f32[256,768]{0,1:T(8,128)}, u32[]{:S(2)}) copy-start(f32[256,768]{0,1:T(8,128)} %copy.20) | copy-start | bytes 2359300
Sparse Core Ops, SparseCore 0:
  9.5 25.2 all-gather.7
  37.6 98.6 all-gather.3
  137.9 20.7 all-gather.5
  173.5 123.0 all-reduce.8
  300.0 119.3 reduce-scatter.4
  422.4 30.4 reduce-scatter.2
where the time goes:
time: 460 us
  waiting for transfers between devices  379 us (82%)
  matrix products  28.4 us (6%)
  other arithmetic  24.1 us (5%)
  between operations  14.3 us (3%)
  local copies, waits for them, and re-layouts  13.4 us (3%)
    reduce_scatter x1, waiting for transfers between devices, shards(): lax.psum_scatter(make_term(saved_rows, grad_proj).astype(jnp.bfloat16), '...  120 us
    all_gather x1, waiting for transfers between devices, shards(): shard_rows = lax.all_gather(weight_both, 'fs', axis=0, tiled=True)  101 us
    psum x1, waiting for transfers between devices, shards(): lax.psum((taps_up_full, taps_gate_full), ('fs', 'tp'))  97.3 us
    reduce_scatter x1, waiting for transfers between devices, shards(): lax.psum_scatter(partial_grad.astype(jnp.bfloat16), 'tp', scatter_dimensi...  29.6 us
    all_gather x1, waiting for transfers between devices, shards(): saved_rows = lax.all_gather(saved_input, 'tp', axis=0, tiled=True)  22.1 us
    unnamed x38, local copies, waits for them, and re-layouts  12.6 us
  transfers between devices with their start and end apart: 6, of which 6 were waited for; matrix products, arithmetic and copies ran while one was open for 11% of the time, Pallas kernels for 0%

commit v1 on v0

--- a/solution.py
+++ b/solution.py
@@ -97,7 +97,7 @@
     taps_gate_full = lax.dynamic_update_slice_in_dim(
         jnp.zeros((3, total_cols), jnp.float32), taps_local[:, column_count:], offset, 1
     )
-    taps_up_total, taps_gate_total = lax.psum((taps_up_full, taps_gate_full), ("fs", "tp"))
+    taps_up_total, taps_gate_total = lax.psum(lax.psum((taps_up_full, taps_gate_full), "tp"), "fs")
     weight_grad = lax.psum_scatter(
         make_term(saved_rows, grad_proj).astype(jnp.bfloat16), "fs", scatter_dimension=0, tiled=True
     ).astype(jnp.float32)

time: 460 us -> 441 us (0.959)
  waiting for transfers between devices: 379 us -> 360 us
    psum x1 -> x2, waiting for transfers between devices: 97.3 us -> 79.6 us  [the longest x1 47.8 us: shards(): lax.psum(lax.psum((taps_up_full, taps_gate_full), 'tp'), 'fs')]
  transfers between devices with their start and end apart: 6 -> 7, of which waited for: 6 -> 7; matrix products, arithmetic and copies ran while one was open for 11% -> 11% of each run, Pallas kernels for 0% -> 0%
where the time goes in v1:
time: 441 us; the launch traced here: 440 us
  waiting for transfers between devices  360 us (82%)
  matrix products  28.4 us (6%)
  other arithmetic  24.2 us (5%)
  between operations  14.4 us (3%)
  local copies, waits for them, and re-layouts  13.4 us (3%)
    reduce_scatter x1, waiting for transfers between devices, shards(): lax.psum_scatter(make_term(saved_rows, grad_proj).astype(jnp.bfloat16), '...  118 us
    all_gather x1, waiting for transfers between devices, shards(): shard_rows = lax.all_gather(weight_both, 'fs', axis=0, tiled=True)  101 us
    psum x1, waiting for transfers between devices, shards(): lax.psum(lax.psum((taps_up_full, taps_gate_full), 'tp'), 'fs')  47.8 us
    psum x1, waiting for transfers between devices, shards(): lax.psum((taps_up_full, taps_gate_full), 'tp')  31.8 us
    reduce_scatter x1, waiting for transfers between devices, shards(): lax.psum_scatter(partial_grad.astype(jnp.bfloat16), 'tp', scatter_dimensi...  29.8 us
    all_gather x1, waiting for transfers between devices, shards(): saved_rows = lax.all_gather(saved_input, 'tp', axis=0, tiled=True)  22.1 us
    unnamed x38, local copies, waits for them, and re-layouts  12.6 us
  transfers between devices with their start and end apart: 7, of which 7 were waited for; matrix products, arithmetic and copies ran while one was open for 11% of the time, Pallas kernels for 0%

profile of v1, /device:TPU:0, one launch (start us, length us, event | category | flops | bytes accessed | tf_op | source)
XLA Modules:
  0.0 440.4 jit_solution(17809762040500614578)
XLA Ops:
  7.2 0.7 all-gather.8.cloned.1.call-update
  8.0 2.0 pad_maximum_fusion.1
  10.1 0.7 all-gather.6.cloned.1.call-update
  10.8 1.2 copy.17
  12.0 0.7 constant_dynamic-slice_fusion
  12.8 22.1 %all-gather.8.cloned.1.call-done = bf16[512,2048]{1,0:T(8,128)(2,1)} async-done(((bf16[128,2048]{1,0:T(8,128)(2,1)}), bf16[512,2048]{1,0:T(8,128)(2,1)}) %all-gather.8.cloned.1.call-update) | async-done | bytes 2097168 | tf_op jit(solution)/shard_map/all_gather | solution.py:69
  34.9 101.5 %all-gather.4.cloned.1.call-done = bf16[2048,1536]{1,0:T(8,128)(2,1)} async-done(((bf16[256,1536]{1,0:T(8,128)(2,1)}), bf16[2048,1536]{1,0:T(8,128)(2,1)}) %all-gather.4.cloned.1.call-update) | async-done | bytes 6291472 | tf_op jit(solution)/shard_map/all_gather | solution.py:70
  136.3 6.2 %convert_bitcast_fusion = f32[512,1536]{0,1:T(8,128)S(1)} fusion(bf16[2048,1536]{1,0:T(8,128)(2,1)} %all-gather.4.cloned.1.call-done, bf16[512,2048]{1,0:T(8,128)(2,1)} %all-gather.8.cloned.1.call-done), kind=kOutput, calls=%fused_computation.9 | convolution fusion | flops 3222798336 | bytes 11534336 | tf_op jit(solution)/shard_map/dot_general | solution.py:72
  142.6 2.6 multiply_add_fusion
  145.3 0.9 fusion.4
  146.2 2.8 fusion.1
  149.0 2.6 fusion.2
  151.6 7.1 %all-gather.6.cloned.1.call-done = bf16[512,2048]{1,0:T(8,128)(2,1)} async-done(((bf16[128,2048]{1,0:T(8,128)(2,1)}), bf16[512,2048]{1,0:T(8,128)(2,1)}) %all-gather.6.cloned.1.call-update) | async-done | bytes 2097168 | tf_op jit(solution)/shard_map/all_gather | solution.py:68
  158.7 6.4 %convert_bitcast_fusion.1 = f32[512,1536]{0,1:T(8,128)S(1)} fusion(bf16[2048,1536]{1,0:T(8,128)(2,1)} %all-gather.4.cloned.1.call-done, bf16[512,2048]{1,0:T(8,128)(2,1)} %all-gather.6.cloned.1.call-done), kind=kOutput, calls=%fused_computation.10 | convolution fusion | flops 3222798336 | bytes 11534336 | tf_op jit(solution)/shard_map/dot_general | solution.py:71
  165.1 7.4 %multiply_reduce_fusion.2 = (f32[1536]{0:T(1024)S(1)}, f32[1536]{0:T(1024)S(1)}, f32[1536]{0:T(1024)S(1)}, bf16[512,1536]{0,1:T(8,128)(2,1)}, f32[512,1536]{0,1:T(8,128)}) fusion(f32[510,1536]{0,1:T(8,128)S(1)} %bitcast.20, f32[512,768]{0,1:T(8,128)S(1)} %copy-done.1, f32[512,768]{0,1:T(8,128)S(1)} %copy-done.3, f32[512,1536]{0,1:T(8,128)S(1)} %convert_bitcast_fusion, ...), kind=kLoop, calls=%fused_computation.13 | loop fusion | flops 14151168 | bytes 33011712 | tf_op jit(solution)/shard_map/reduce_sum | solution.py:28
  172.7 0.6 copy-done.13
  173.4 31.8 %all-reduce.13.cloned.1.call-done = (f32[3,3072]{1,0:T(4,128)}, f32[3,3072]{1,0:T(4,128)}) async-done(((f32[3,3072]{1,0:T(4,128)}, f32[3,3072]{1,0:T(4,128)}), (f32[3,3072]{1,0:T(4,128)}, f32[3,3072]{1,0:T(4,128)})) %all-reduce.13.cloned.1.call-update) | async-done | bytes 73744 | tf_op jit(solution)/shard_map/psum | solution.py:100
  205.5 8.2 %fusion = bf16[2048,1536]{0,1:T(8,128)(2,1)} fusion(bf16[512,1536]{0,1:T(8,128)(2,1)} %get-tuple-element.24, bf16[512,2048]{1,0:T(8,128)(2,1)} %all-gather.8.cloned.1.call-done), kind=kOutput, calls=%fused_computation.1 | convolution fusion | flops 3224371200 | bytes 9961472 | tf_op jit(solution)/shard_map/dot_general | solution.py:37
  213.8 1.3 copy-done.10
  215.1 7.6 %convolution_convert_fusion.1 = bf16[512,2048]{1,0:T(8,128)(2,1)} fusion(bf16[512,1536]{0,1:T(8,128)(2,1)S(1)} %copy-done.10, bf16[2048,1536]{1,0:T(8,128)(2,1)} %all-gather.4.cloned.1.call-done), kind=kOutput, calls=%fused_computation.17 | convolution fusion | flops 3222274048 | bytes 9961472 | tf_op jit(solution)/shard_map/dot_general | solution.py:106
  222.7 2.5 copy.19
  225.2 2.3 copy.20
  227.5 1.4 fusion.5
  228.8 2.4 copy.21
  231.2 47.8 %all-reduce.11.cloned.1.call-done = (f32[3,3072]{1,0:T(4,128)}, f32[3,3072]{1,0:T(4,128)}) async-done(((f32[3,3072]{1,0:T(4,128)}, f32[3,3072]{1,0:T(4,128)}), (f32[3,3072]{1,0:T(4,128)}, f32[3,3072]{1,0:T(4,128)})) %all-reduce.11.cloned.1.call-update) | async-done | bytes 73744 | tf_op jit(solution)/shard_map/psum | solution.py:100
  279.0 1.4 multiply_add_fusion.2
  280.5 1.4 multiply_add_fusion.3
  281.9 118.1 %reduce-scatter.5.cloned.1.call-done = bf16[256,1536]{0,1:T(8,128)(2,1)} async-done(((bf16[2048,1536]{0,1:T(8,128)(2,1)}), bf16[256,1536]{0,1:T(8,128)(2,1)}) %reduce-scatter.5.cloned.1.call-update) | async-done | bytes 786448 | tf_op jit(solution)/shard_map/reduce_scatter | solution.py:101
  400.0 1.2 convert_element_type.57
  401.5 1.1 copy.22
  402.7 1.1 copy.23
  403.8 29.8 %reduce-scatter.3.cloned.1.call-done = bf16[128,2048]{1,0:T(8,128)(2,1)} async-done(((bf16[512,2048]{1,0:T(8,128)(2,1)}), bf16[128,2048]{1,0:T(8,128)(2,1)}) %reduce-scatter.3.cloned.1.call-update) | async-done | bytes 524304 | tf_op jit(solution)/shard_map/reduce_scatter | solution.py:112
  (52 shorter events, 1.0 us)
Async XLA Ops:
  7.2 3.7 copy-start.11
  7.2 27.7 %all-gather.8.cloned.1.call-start = ((), (), s32[]{:S(2)}) async-start(), calls=%async_computation.4 | async-start | bytes 2621440 | tf_op jit(solution)/shard_map/all_gather | solution.py:69
  7.9 128.4 %all-gather.4.cloned.1.call-start = ((), (), s32[]{:S(2)}) async-start(), calls=%async_computation.2 | async-start | bytes 7077888 | tf_op jit(solution)/shard_map/all_gather | solution.py:70
  10.0 148.7 %all-gather.6.cloned.1.call-start = ((), (), s32[]{:S(2)}) async-start(), calls=%async_computation.3 | async-start | bytes 2621440 | tf_op jit(solution)/shard_map/all_gather | solution.py:68
  10.8 194.5 %all-reduce.13.cloned.1.call-start = ((), (), s32[]{:S(2)}) async-start(), calls=%async_computation.8 | async-start | bytes 196608 | tf_op jit(solution)/shard_map/psum | solution.py:100
  142.6 2.7 copy-start.9
  146.2 2.8 copy-start
  146.2 2.8 copy-start.2
  158.7 6.4 %copy-start.1 = (f32[512,768]{0,1:T(8,128)S(1)}, f32[512,768]{0,1:T(8,128)}, u32[]{:S(2)}) copy-start(f32[512,768]{0,1:T(8,128)} %copy-done) | copy-start | bytes 4718596
  158.7 6.4 %copy-start.3 = (f32[512,768]{0,1:T(8,128)S(1)}, f32[512,768]{0,1:T(8,128)}, u32[]{:S(2)}) copy-start(f32[512,768]{0,1:T(8,128)} %copy-done.2) | copy-start | bytes 4718596
  158.7 6.4 %copy-start.4 = (f32[511,1536]{0,1:T(8,128)S(1)}, f32[511,1536]{0,1:T(8,128)}, u32[]{:S(2)}) copy-start(f32[511,1536]{0,1:T(8,128)} %fusion.1) | copy-start | bytes 9418756
  158.7 6.4 %copy-start.5 = (f32[510,1536]{0,1:T(8,128)S(1)}, f32[510,1536]{0,1:T(8,128)}, u32[]{:S(2)}) copy-start(f32[510,1536]{0,1:T(8,128)} %fusion.2) | copy-start | bytes 9400324
  172.7 0.6 copy-start.13
  172.7 0.6 copy-start.12
  173.4 105.7 %all-reduce.11.cloned.1.call-start = ((), (), s32[]{:S(2)}) async-start(), calls=%async_computation.7 | async-start | bytes 196608 | tf_op jit(solution)/shard_map/psum | solution.py:100
  205.3 194.8 %reduce-scatter.5.cloned.1.call-start = ((), (), s32[]{:S(2)}) async-start(), calls=%async_computation.6 | async-start | bytes 7077888 | tf_op jit(solution)/shard_map/reduce_scatter | solution.py:101
  213.7 1.4 copy-start.10
  213.7 219.9 %reduce-scatter.3.cloned.1.call-start = ((), (), s32[]{:S(2)}) async-start(), calls=%async_computation.5 | async-start | bytes 2621440 | tf_op jit(solution)/shard_map/reduce_scatter | solution.py:112
  222.7 4.8 %copy-start.6 = (f32[512,1536]{0,1:T(8,128)S(1)}, f32[512,1536]{0,1:T(8,128)}, u32[]{:S(2)}) copy-start(f32[512,1536]{0,1:T(8,128)} %get-tuple-element.27) | copy-start | bytes 9437188
  227.4 51.6 %copy-start.14 = (f32[3,3072]{1,0:T(4,128)S(1)}, f32[3,3072]{1,0:T(4,128)}, u32[]{:S(2)}) copy-start(f32[3,3072]{1,0:T(4,128)} %param.21) | copy-start | bytes 110596
  227.4 53.0 %copy-start.15 = (f32[3,3072]{1,0:T(4,128)S(1)}, f32[3,3072]{1,0:T(4,128)}, u32[]{:S(2)}) copy-start(f32[3,3072]{1,0:T(4,128)} %param.20) | copy-start | bytes 110596
  228.8 172.5 %copy-start.7 = (f32[256,768]{0,1:T(8,128)S(1)}, f32[256,768]{0,1:T(8,128)}, u32[]{:S(2)}) copy-start(f32[256,768]{0,1:T(8,128)} %copy.19) | copy-start | bytes 2359300
  228.8 172.5 %copy-start.8 = (f32[256,768]{0,1:T(8,128)S(1)}, f32[256,768]{0,1:T(8,128)}, u32[]{:S(2)}) copy-start(f32[256,768]{0,1:T(8,128)} %copy.20) | copy-start | bytes 2359300
Sparse Core Ops, SparseCore 0:
  9.5 25.2 all-gather.7
  37.6 98.6 all-gather.3
  137.9 20.7 all-gather.5
  173.5 31.7 all-reduce.12
  208.5 70.4 all-reduce.10
  282.5 117.4 reduce-scatter.4
  403.1 30.4 reduce-scatter.2
